TPU v7x, 256 devices: a whole 4x4x8 slice. The times are simulated.
256 devices in a mesh: ep: 64 (over z, y, core), tp: 4 (over x).
Axes of the slice: x: 4, y: 4, z: 8, core: 2. Of those that a mesh axis runs over, the one named last changes fastest.
Arguments:
- mixer_input: bfloat16 [32768, 2048], P('ep'), may hold values from -6 to 6
- mixer_gain: bfloat16 [2048], replicated, may hold values from 0.099609375 to 1.8984375
- pool_in: bfloat16 [2048, 1024], P(None, 'tp'), may hold values from -0.125 to 0.125
- pool_map: bfloat16 [4, 256, 256], P('tp'), may hold values from -0.375 to 0.375
- pool_scale: bfloat16 [1024], P('tp'), may hold values from 0.099609375 to 1.8984375
- pool_out: bfloat16 [1024, 2048], P('tp'), may hold values from -0.1875 to 0.1875
- expert_input: bfloat16 [24576, 2048], P('ep'), may hold values from -6 to 6
- expert_gain: bfloat16 [2048], replicated, may hold values from 0.099609375 to 1.8984375
- group_router: bfloat16 [2048, 4], replicated, may hold values from -0.125 to 0.125
- expert_router: bfloat16 [2048, 64], replicated, may hold values from -0.125 to 0.125
- routes: int32 [24576, 2], P('ep'), may hold values from 0 to 63, all different within a row; in each aligned block of 96 rows (0 to 95, 96 to 191, ...) at most 6 rows name the same one
- gate_weight: bfloat16 [64, 2048, 1024], P('ep', None, 'tp'), may hold values from -0.125 to 0.125
- up_weight: bfloat16 [64, 2048, 1024], P('ep', None, 'tp'), may hold values from -0.125 to 0.125
- down_weight: bfloat16 [64, 1024, 2048], P('ep', 'tp'), may hold values from -0.1875 to 0.1875
Outputs:
- mixer_output: bfloat16 [32768, 2048], P(('ep', 'tp'))
- expert_output: bfloat16 [24576, 2048], P(('ep', 'tp'))
Inputs may be any that keep to these rules, and one draw needn't show every extreme that they name: `routes`: each row names two different experts. In each aligned block of 96 rows no expert is named more than 6 times, a bound that some block reaches.
All inputs are finite; a program needn't handle non-finite values.
Results may differ from a plain program's by a relative error of at most 0.01.
Values may be sent and summed in bfloat16 or wider, within the bound.
No kernel may reach another device: no remote copies, remote signals or barrier semaphores. Data moves between devices by JAX's collectives and lax.ppermute only.
A program may use at most 64 MiB of HBM per device.

v0:
```python
import jax
import jax.numpy as jnp
from jax import lax
from jax.sharding import PartitionSpec as P

RIM = 15
EPS = 1e-06


def passed_along(value, axis, steps):
    count = lax.axis_size(axis)
    leading, last = (max(0, -steps), min(count, count - steps))
    return lax.ppermute(value, axis, [(source, source + steps) for source in range(leading, last)])


def norm_rows(values, gain):
    floats = values.astype(jnp.float32)
    scale = lax.rsqrt(jnp.mean(floats * floats, axis=-1, keepdims=True) + EPS)
    return (floats * scale * gain.astype(jnp.float32)).astype(jnp.bfloat16)


def route_weights(rows, group_router, expert_router, route_rows):
    group_logits = jnp.dot(rows, group_router, preferred_element_type=jnp.float32)
    expert_logits = jnp.dot(rows, expert_router, preferred_element_type=jnp.float32)
    groups = group_logits.shape[1]
    experts = expert_logits.shape[1]
    member = (
        jnp.arange(experts, dtype=jnp.int32)[:, None] // (experts // groups)
        == jnp.arange(groups, dtype=jnp.int32)[None, :]
    ).astype(jnp.float32)
    group_exp = jnp.exp(group_logits)
    group_prob = group_exp / jnp.sum(group_exp, axis=1, keepdims=True)
    expert_exp = jnp.exp(expert_logits)
    within = jnp.dot(expert_exp, member, precision=lax.Precision.HIGHEST)
    prob = expert_exp * jnp.dot(group_prob / within, member.T, precision=lax.Precision.HIGHEST)
    chosen = (route_rows[:, :, None] == jnp.arange(experts, dtype=jnp.int32)[None, None, :]).astype(
        jnp.float32
    )
    picked = jnp.sum(chosen * prob[:, None, :], axis=2)
    return picked / jnp.sum(picked, axis=1, keepdims=True)


def mixer_half(mixer_input, mixer_gain, pool_in, pool_map, pool_scale, pool_out):
    normed = norm_rows(mixer_input, mixer_gain)
    pooled_in = jnp.dot(normed, pool_in, preferred_element_type=jnp.float32).astype(jnp.bfloat16)
    local_rows = pooled_in.shape[0]
    groups_here = pool_map.shape[0]
    channels = pool_map.shape[1]
    border = passed_along(pooled_in[local_rows - RIM :], "ep", 1)
    padded = jnp.concatenate([border, pooled_in], axis=0).astype(jnp.float32)
    padded = padded.reshape(local_rows + RIM, groups_here, channels)
    leading = lax.axis_index("tp") * groups_here
    windows = jnp.left_shift(jnp.int32(2), leading + jnp.arange(groups_here, dtype=jnp.int32))
    window_sum = jnp.zeros((local_rows, groups_here, channels), jnp.float32)
    for offset in range(RIM + 1):
        active = (offset < windows).astype(jnp.float32)
        window_sum = (
            window_sum + padded[RIM - offset : RIM - offset + local_rows] * active[None, :, None]
        )
    position = lax.axis_index("ep") * local_rows + jnp.arange(local_rows, dtype=jnp.int32)
    counts_here = jnp.minimum(position[:, None] + 1, windows[None, :]).astype(jnp.float32)
    pooled = (window_sum / counts_here[:, :, None] - padded[RIM:]).astype(jnp.bfloat16)
    mapped = jnp.einsum("tgc,gce->tge", pooled, pool_map, preferred_element_type=jnp.float32)
    mixed_rows = (
        mapped.reshape(local_rows, groups_here * channels) * pool_scale.astype(jnp.float32)
    ).astype(jnp.bfloat16)
    return lax.psum_scatter(
        jnp.dot(mixed_rows, pool_out, preferred_element_type=jnp.float32).astype(jnp.bfloat16),
        "tp",
        scatter_dimension=0,
        tiled=True,
    )


def slot_positions(route_rows, blocks, experts):
    flat = route_rows.reshape(blocks, -1)
    onehot = (flat[:, :, None] == jnp.arange(experts, dtype=jnp.int32)[None, None, :]).astype(
        jnp.int32
    )
    before = jnp.cumsum(onehot, axis=1) - onehot
    return (jnp.sum(before * onehot, axis=2), flat)


def dispatch_rows(normed, route_rows, blocks, slots_each, experts):
    block_len = normed.shape[0] // blocks
    positions, flat = slot_positions(route_rows, blocks, experts)
    block_index = jnp.arange(blocks, dtype=jnp.int32)[:, None]
    slot_index = block_index * slots_each + positions
    token_index = block_index * block_len + jnp.arange(2 * block_len, dtype=jnp.int32)[None, :] // 2
    table = jnp.full((blocks * slots_each, experts), -1, jnp.int32)
    table = table.at[slot_index.reshape(-1), flat.reshape(-1)].set(token_index.reshape(-1))
    fetched = normed[jnp.maximum(table, 0)]
    return jnp.where((table >= 0)[:, :, None], fetched, jnp.zeros_like(fetched))


def expert_half(
    expert_input,
    expert_gain,
    group_router,
    expert_router,
    routes,
    gate_weight,
    up_weight,
    down_weight,
):
    normed = norm_rows(expert_input, expert_gain)
    tp_count = lax.axis_size("tp")
    tp_place = lax.axis_index("tp")
    experts = expert_router.shape[1]
    block_len = normed.shape[0] // tp_count
    slots_each = 4 * block_len // experts
    own_rows = lax.dynamic_slice_in_dim(normed, tp_place * block_len, block_len, 0)
    own_routes = lax.dynamic_slice_in_dim(routes, tp_place * block_len, block_len, 0)
    sending = dispatch_rows(own_rows, own_routes, 1, slots_each, experts)
    arrived = lax.all_to_all(sending, "ep", split_axis=1, concat_axis=1, tiled=True)
    received = lax.all_gather(arrived, "tp", axis=0, tiled=True)
    held = gate_weight.shape[0]
    model = received.shape[2]
    down_whole = lax.all_gather(down_weight, "tp", axis=1, tiled=True)
    all_slots = received.reshape(received.shape[0], -1, held, model)
    gate = jnp.einsum("csed,edh->cseh", all_slots, gate_weight, preferred_element_type=jnp.float32)
    upward = jnp.einsum("csed,edh->cseh", all_slots, up_weight, preferred_element_type=jnp.float32)
    hidden = (jax.nn.silu(gate) * upward).astype(jnp.bfloat16)
    swapped = lax.all_to_all(hidden, "tp", split_axis=0, concat_axis=3, tiled=True)
    hid_part = hidden.shape[3]
    total = jnp.zeros((swapped.shape[0], swapped.shape[1], held, model), jnp.float32)
    for part in range(tp_count):
        partial_value = jnp.einsum(
            "cseh,ehd->csed",
            swapped[:, :, :, part * hid_part : (part + 1) * hid_part],
            down_whole[:, part * hid_part : (part + 1) * hid_part],
            preferred_element_type=jnp.float32,
        ).astype(jnp.bfloat16)
        partial_value = lax.optimization_barrier(partial_value)
        total = total + partial_value.astype(jnp.float32)
    summed = total.astype(jnp.bfloat16).reshape(slots_each, -1, model)
    returned = lax.all_to_all(summed, "ep", split_axis=1, concat_axis=1, tiled=True)
    positions, flat = slot_positions(own_routes, 1, experts)
    lookup = positions[0] * experts + flat[0]
    picked = (
        returned.reshape(slots_each * experts, model)[lookup]
        .astype(jnp.float32)
        .reshape(block_len, 2, model)
    )
    weights = route_weights(own_rows, group_router, expert_router, own_routes)
    return jnp.sum(picked * weights[:, :, None], axis=1).astype(jnp.bfloat16)


def on_device(
    mixer_input,
    mixer_gain,
    pool_in,
    pool_map,
    pool_scale,
    pool_out,
    expert_input,
    expert_gain,
    group_router,
    expert_router,
    routes,
    gate_weight,
    up_weight,
    down_weight,
):
    mixer_output = mixer_half(mixer_input, mixer_gain, pool_in, pool_map, pool_scale, pool_out)
    expert_output = expert_half(
        expert_input,
        expert_gain,
        group_router,
        expert_router,
        routes,
        gate_weight,
        up_weight,
        down_weight,
    )
    return (mixer_output, expert_output)


def solution(mesh):
    return jax.shard_map(
        on_device,
        mesh=mesh,
        in_specs=(
            P("ep", None),
            P(),
            P(None, "tp"),
            P("tp", None, None),
            P("tp"),
            P("tp", None),
            P("ep", None),
            P(),
            P(),
            P(),
            P("ep", None),
            P("ep", None, "tp"),
            P("ep", None, "tp"),
            P("ep", "tp", None),
        ),
        out_specs=(P(("ep", "tp"), None), P(("ep", "tp"), None)),
        check_vma=False,
    )
```

profile of v0, /device:TPU:8, one launch (start us, length us, event | category | flops | bytes accessed | tf_op | source)
XLA Modules:
  0.0 302.8 jit_solution(5306408200580199578)
XLA Ops:
  7.2 0.9 constant_dynamic-slice_fusion
  9.5 1.8 multiply_reduce_fusion
  11.3 2.0 convert_element_type.227
  13.9 9.3 %scatter_fusion = s32[6,64]{1,0:T(8,128)S(1)} fusion(s32[6,64]{1,0:T(8,128)S(1)} %broadcast_in_dim.11, s32[192]{0:T(256)S(1)} %bitcast.129, s32[192]{0:T(256)S(1)} %and_select_fusion.1), kind=kCustom, calls=%fused_computation.2 | custom fusion | bytes 3840 | tf_op jit(solution)/shard_map/scatter | solution.py:91
  23.5 1.3 fusion.26
  24.8 2.5 gather_fusion
  27.2 1.0 copy_select_fusion
  28.2 63.1 %all_to_all.28 = bf16[6,64,2048]{2,0,1:T(8,128)(2,1)S(1)} all-to-all(bf16[6,64,2048]{2,0,1:T(8,128)(2,1)S(1)} %copy_select_fusion), channel_id=1, replica_groups=mesh['ep'=64,'tp'=4] {'ep'}, dimensions={1} | all-to-all | bytes 3145728 | tf_op jit(solution)/shard_map/all_to_all | solution.py:115
  91.4 2.0 copy.48
  93.5 0.7 all-gather.5.cloned.1.call-update
  94.2 0.8 copy-done.3
  95.6 0.8 fusion.17
  96.4 0.7 copy-done.4
  97.1 1.9 collective-permute-start
  99.1 58.8 %all-gather.3.cloned.1.call-done = bf16[24,64,2048]{2,1,0:T(8,128)(2,1)} async-done(((bf16[6,64,2048]{2,1,0:T(8,128)(2,1)}), bf16[24,64,2048]{2,1,0:T(8,128)(2,1)}) %all-gather.3.cloned.1.call-update) | async-done | bytes 6291472 | tf_op jit(solution)/shard_map/all_gather | solution.py:116
  157.9 5.1 %fusion.23 = f32[24,64,256]{2,1,0:T(8,128)S(1)} fusion(bf16[24,64,2048]{2,1,0:T(8,128)(2,1)} %all-gather.3.cloned.1.call-done, bf16[1,2048,256]{2,1,0:T(8,128)(2,1)} %param.25), kind=kOutput, calls=%fused_computation.46 | convolution fusion | flops 1610612736 | bytes 8912896 | tf_op jit(solution)/shard_map/csed,edh->cseh/dot_general | solution.py:121
  163.1 3.0 fusion.16
  166.1 3.8 %all-to-all-start.1 = ((bf16[24,64,1,256]{3,1,2,0:T(8,128)(2,1)}), bf16[24,64,1,256]{3,1,2,0:T(8,128)(2,1)S(1)}, u32[]{:S(2)}, u32[]{:S(2)}) async-start(bf16[24,64,1,256]{3,1,2,0:T(8,128)(2,1)} %fusion.16), calls=%async_computation.2 | async-start | bytes 1572864 | tf_op jit(solution)/shard_map/all_to_all | solution.py:124
  170.0 3.3 %convolution_convert_fusion = bf16[512,2048]{1,0:T(8,128)(2,1)} fusion(bf16[256,2048]{1,0:T(8,128)(2,1)S(1)} %copy-done, f32[256]{0:T(256)S(1)} %convert_element_type.223, f32[527,256]{1,0:T(8,128)S(1)} %maximum_convert_fusion, f32[512]{0:T(512)S(1)} %minimum_convert_fusion, f32[]{:T(128)S(6)} %convert_element_type.220, f32[]{:T(128)S(6)} %convert_element_type.219, ...), kind=kOutput, calls=%fused_computation.10 | convolution fusion | flops 609746944 | bytes 11668544 | tf_op jit(solution)/shard_map/dot_general | solution.py:68
  173.4 14.8 %all-to-all-done.1 = bf16[24,64,1,256]{3,1,2,0:T(8,128)(2,1)S(1)} async-done(((bf16[24,64,1,256]{3,1,2,0:T(8,128)(2,1)}), bf16[24,64,1,256]{3,1,2,0:T(8,128)(2,1)S(1)}, u32[]{:S(2)}, u32[]{:S(2)}) %all-to-all-start.1) | async-done | bytes 786464 | tf_op jit(solution)/shard_map/all_to_all | solution.py:124
  188.2 0.6 copy.56
  189.4 26.5 %all-gather.5.cloned.1.call-done = bf16[1,1024,2048]{2,1,0:T(8,128)(2,1)} async-done(((bf16[1,256,2048]{2,1,0:T(8,128)(2,1)}), bf16[1,1024,2048]{2,1,0:T(8,128)(2,1)}) %all-gather.5.cloned.1.call-update) | async-done | bytes 4194320 | tf_op jit(solution)/shard_map/all_gather | solution.py:119
  215.8 2.0 fusion.3
  217.8 1.8 fusion.4
  220.8 1.4 fusion.11
  222.2 2.2 copy.51
  224.4 10.9 %all-to-all-start.2 = ((bf16[6,64,2048]{2,0,1:T(8,128)(2,1)}), bf16[6,64,2048]{2,0,1:T(8,128)(2,1)}, u32[]{:S(2)}, u32[]{:S(2)}) async-start(bf16[6,64,2048]{2,0,1:T(8,128)(2,1)} %copy.51), calls=%async_computation.3 | async-start | bytes 4194304 | tf_op jit(solution)/shard_map/all_to_all | solution.py:137
  236.5 49.9 %all-to-all-done.2 = bf16[6,64,2048]{2,0,1:T(8,128)(2,1)} async-done(((bf16[6,64,2048]{2,0,1:T(8,128)(2,1)}), bf16[6,64,2048]{2,0,1:T(8,128)(2,1)}, u32[]{:S(2)}, u32[]{:S(2)}) %all-to-all-start.2) | async-done | bytes 1572896 | tf_op jit(solution)/shard_map/all_to_all | solution.py:137
  286.4 2.5 copy.52
  288.9 2.1 gather_fusion.1
  290.9 2.1 reshape.556
  293.1 3.1 %multiply_reduce_fusion.1 = bf16[96,2048]{1,0:T(8,128)(2,1)} fusion(f32[96,2,2048]{2,1,0:T(2,128)S(1)} %reshape.556, f32[96,2]{1,0:T(8,128)S(1)} %copy.53), kind=kLoop, calls=%fused_computation.31 | loop fusion | flops 589824 | bytes 1966848 | tf_op jit(solution)/shard_map/reduce_sum | solution.py:146
  (80 shorter events, 6.0 us)
Async XLA Ops:
  7.2 162.9 %copy-start = (bf16[256,2048]{1,0:T(8,128)(2,1)S(1)}, bf16[256,2048]{1,0:T(8,128)(2,1)}, u32[]{:S(2)}) copy-start(bf16[256,2048]{1,0:T(8,128)(2,1)} %param.19) | copy-start | bytes 3145732
  7.2 4.2 %copy-start.1 = (bf16[384,2048]{1,0:T(8,128)(2,1)S(1)}, bf16[384,2048]{1,0:T(8,128)(2,1)}, u32[]{:S(2)}) copy-start(bf16[384,2048]{1,0:T(8,128)(2,1)} %param.20) | copy-start | bytes 4718596
  7.2 150.7 %all-gather.3.cloned.1.call-start = ((), (), s32[]{:S(2)}) async-start(), calls=%async_computation.5 | async-start | bytes 7864320 | tf_op jit(solution)/shard_map/all_gather | solution.py:116
  13.4 10.0 %copy-start.8 = (bf16[2048]{0:T(1024)(128)(2,1)S(1)}, bf16[2048]{0:T(1024)(128)(2,1)}, u32[]{:S(2)}) copy-start(bf16[2048]{0:T(1024)(128)(2,1)} %param.21) | copy-start | bytes 12292
  93.4 0.8 copy-start.9
  93.4 1.6 copy-start.3
  93.4 122.4 %all-gather.5.cloned.1.call-start = ((), (), s32[]{:S(2)}) async-start(), calls=%async_computation.6 | async-start | bytes 5242880 | tf_op jit(solution)/shard_map/all_gather | solution.py:119
  94.2 1.4 copy-start.11
  95.6 3.5 %copy-start.14 = (bf16[256]{0:T(256)(128)(2,1)S(1)}, bf16[256]{0:T(256)(128)(2,1)}, u32[]{:S(2)}) copy-start(bf16[256]{0:T(256)(128)(2,1)} %param.18) | copy-start | bytes 1540
  96.4 0.7 copy-start.4
  97.1 72.9 %collective-permute-start = (bf16[15,256]{1,0:T(8,128)(2,1)S(1)}, bf16[15,256]{1,0:T(8,128)(2,1)S(1)}, u32[]{:S(2)}, u32[]{:S(2)}) collective-permute-start(bf16[15,256]{1,0:T(8,128)(2,1)S(1)} %slice.135), channel_id=1, source_target_pairs={{0,4},{4,8},{8,12},{12,16},{16,20},{20,24},{24,28},{28,32},{32,36}... | collective-permute-start | bytes 23048 | tf_op jit(solution)/shard_map/ppermute | solution.py:13
  157.9 5.1 %copy-start.10 = (bf16[24,64,2048]{2,1,0:T(8,128)(2,1)S(1)}, bf16[24,64,2048]{2,1,0:T(8,128)(2,1)}, u32[]{:S(2)}) copy-start(bf16[24,64,2048]{2,1,0:T(8,128)(2,1)} %all-gather.3.cloned.1.call-done) | copy-start | bytes 18874372
  157.9 5.1 %copy-start.12 = (bf16[1,2048,256]{2,1,0:T(8,128)(2,1)S(1)}, bf16[1,2048,256]{2,1,0:T(8,128)(2,1)}, u32[]{:S(2)}) copy-start(bf16[1,2048,256]{2,1,0:T(8,128)(2,1)} %param.26) | copy-start | bytes 3145732
  163.1 6.9 %copy-start.5 = (bf16[512,256]{1,0:T(8,128)(2,1)S(1)}, bf16[512,256]{1,0:T(8,128)(2,1)}, u32[]{:S(2)}) copy-start(bf16[512,256]{1,0:T(8,128)(2,1)} %copy-done.4) | copy-start | bytes 786436
  166.1 4.0 %copy-start.13 = (bf16[1,256,256]{2,1,0:T(8,128)(2,1)S(1)}, bf16[1,256,256]{2,1,0:T(8,128)(2,1)}, u32[]{:S(2)}) copy-start(bf16[1,256,256]{2,1,0:T(8,128)(2,1)} %param.17) | copy-start | bytes 393220
  166.1 22.1 %all-to-all-start.1 = ((bf16[24,64,1,256]{3,1,2,0:T(8,128)(2,1)}), bf16[24,64,1,256]{3,1,2,0:T(8,128)(2,1)S(1)}, u32[]{:S(2)}, u32[]{:S(2)}) async-start(bf16[24,64,1,256]{3,1,2,0:T(8,128)(2,1)} %fusion.16), calls=%async_computation.2 | async-start | bytes 1572864 | tf_op jit(solution)/shard_map/all_to_all | solution.py:124
  169.9 126.4 %reduce-scatter.2.cloned.1.call-start = ((), (), s32[]{:S(2)}) async-start(), calls=%async_computation.4 | async-start | bytes 2621440 | tf_op jit(solution)/shard_map/reduce_scatter | solution.py:67
  215.8 3.8 %copy-start.2 = (bf16[1,1024,2048]{2,1,0:T(8,128)(2,1)S(1)}, bf16[1,1024,2048]{2,1,0:T(8,128)(2,1)}, u32[]{:S(2)}) copy-start(bf16[1,1024,2048]{2,1,0:T(8,128)(2,1)} %all-gather.5.cloned.1.call-done) | copy-start | bytes 12582916
  224.4 10.9 %copy-start.7 = (bf16[2048,4]{0,1:T(4,128)(2,1)S(1)}, bf16[2048,4]{0,1:T(4,128)(2,1)}, u32[]{:S(2)}) copy-start(bf16[2048,4]{0,1:T(4,128)(2,1)} %param.22) | copy-start | bytes 49156
  224.4 11.2 %copy-start.6 = (bf16[2048,64]{0,1:T(8,128)(2,1)S(1)}, bf16[2048,64]{0,1:T(8,128)(2,1)}, u32[]{:S(2)}) copy-start(bf16[2048,64]{0,1:T(8,128)(2,1)} %param.23) | copy-start | bytes 786436
  224.4 62.0 %all-to-all-start.2 = ((bf16[6,64,2048]{2,0,1:T(8,128)(2,1)}), bf16[6,64,2048]{2,0,1:T(8,128)(2,1)}, u32[]{:S(2)}, u32[]{:S(2)}) async-start(bf16[6,64,2048]{2,0,1:T(8,128)(2,1)} %copy.51), calls=%async_computation.3 | async-start | bytes 4194304 | tf_op jit(solution)/shard_map/all_to_all | solution.py:137
Sparse Core Ops, SparseCore 0:
  93.5 64.3 all-gather.2
  159.7 56.0 all-gather.4
  219.0 31.9 reduce-scatter.1
where the time goes:
time: 303 us
  waiting for transfers between devices  151 us (50%)
  blocking collectives  63.1 us (21%)
  local copies, waits for them, and re-layouts  27.7 us (9%)
  matrix products  18 us (6%)
  starting transfers between devices  16.7 us (6%)
  between operations  14.2 us (5%)
  other arithmetic  12.1 us (4%)
    all_to_all x1, blocking collectives, expert_half(): lax.all_to_all(sending, 'ep', split_axis=1, concat_axis=1, tiled=True)  63.1 us
    all_gather x1, waiting for transfers between devices, expert_half(): received = lax.all_gather(arrived, 'tp', axis=0, tiled=True)  58.8 us
    all_to_all x1, waiting for transfers between devices, expert_half(): lax.all_to_all(summed, 'ep', split_axis=1, concat_axis=1, tiled=True)  49.9 us
    all_gather x1, waiting for transfers between devices, expert_half(): down_whole = lax.all_gather(down_weight, 'tp', axis=1, tiled=True)  26.5 us
    all_to_all x1, waiting for transfers between devices, expert_half(): lax.all_to_all(hidden, 'tp', split_axis=0, concat_axis=3, tiled=True)  14.8 us
    all_to_all x1, starting transfers between devices, expert_half(): lax.all_to_all(summed, 'ep', split_axis=1, concat_axis=1, tiled=True)  10.9 us
    scatter x1, local copies, waits for them, and re-layouts, dispatch_rows(): table.at[slot_index.reshape(-1), flat.reshape(-1)]  9.28 us
  transfers between devices with their start and end apart: 6, of which 4 were waited for; matrix products, arithmetic and copies ran while one was open for 11% of the time, Pallas kernels for 0%

commit v1 on v0

--- a/solution.py
+++ b/solution.py
@@ -1,3 +1,4 @@
+import functools
 import jax
 import jax.numpy as jnp
 from jax import lax
@@ -5,6 +6,33 @@
 
 RIM = 15
 EPS = 1e-06
+
+
+def slots_press(z_in, pos_dim):
+    z_in = jnp.moveaxis(z_in, 0, pos_dim)
+    g_now = z_in.shape
+    return z_in.reshape(
+        *g_now[:pos_dim], g_now[pos_dim] * g_now[pos_dim + 1], *g_now[pos_dim + 2 :]
+    )
+
+
+def apply_limits(block_in, axis_name, on_dim):
+    dev_n = lax.axis_size(axis_name)
+    sheets = list(map(lambda dev_i: (dev_i, (dev_i + 1) % dev_n), range(dev_n)))
+    in_order = [(num, w) for w, num in sheets]
+    near, z2 = ([], [])
+    for pp in range(dev_n - 1):
+        if pp % 2 == 0:
+            near.append(lax.ppermute(near[-1] if near else block_in, axis_name, sheets))
+        else:
+            z2.append(lax.ppermute(z2[-1] if z2 else block_in, axis_name, in_order))
+    oldest = jnp.stack([*near[::-1], block_in, *z2], axis=0)
+    passed = lax.axis_index(axis_name) - len(near)
+    oldest = oldest[(jnp.arange(dev_n) - passed) % dev_n]
+    return slots_press(oldest, on_dim)
+
+
+pack_pools = functools.partial(apply_limits, axis_name="tp", on_dim=1)
 
 
 def passed_along(value, axis, steps):
@@ -116,7 +144,7 @@
     received = lax.all_gather(arrived, "tp", axis=0, tiled=True)
     held = gate_weight.shape[0]
     model = received.shape[2]
-    down_whole = lax.all_gather(down_weight, "tp", axis=1, tiled=True)
+    down_whole = pack_pools(down_weight)
     all_slots = received.reshape(received.shape[0], -1, held, model)
     gate = jnp.einsum("csed,edh->cseh", all_slots, gate_weight, preferred_element_type=jnp.float32)
     upward = jnp.einsum("csed,edh->cseh", all_slots, up_weight, preferred_element_type=jnp.float32)

time: 303 us -> 303 us (level)
  waiting for transfers between devices: 151 us -> 138 us
  local copies, waits for them, and re-layouts: 27.7 us -> 32.8 us
  other arithmetic: 12.1 us -> 16.6 us
    ppermute x0 -> x3, waiting for transfers between devices: none -> 28.8 us  [the longest x2 28.8 us: apply_limits(): near.append(lax.ppermute(near[-1] if near else block_in, axis_name, sheets))]
    all_gather x1 -> x0, waiting for transfers between devices: 26.5 us -> none  [expert_half(): down_whole = lax.all_gather(down_weight, 'tp', axis=1, tiled=True)]
    all_to_all x1, waiting for transfers between devices: 14.8 us -> 0.01 us  [expert_half(): lax.all_to_all(hidden, 'tp', split_axis=0, concat_axis=3, tiled=True)]
    gather x0 -> x1, local copies, waits for them, and re-layouts: none -> 4.97 us  [apply_limits(): oldest = oldest[(jnp.arange(dev_n) - passed) % dev_n]]
    ppermute x0 -> x3, starting transfers between devices: none -> 4.94 us  [the longest x2 3.2 us: apply_limits(): near.append(lax.ppermute(near[-1] if near else block_in, axis_name, sheets))]
    all_to_all x1, starting transfers between devices: 10.9 us -> 7.18 us  [expert_half(): lax.all_to_all(summed, 'ep', split_axis=1, concat_axis=1, tiled=True)]
    another operation x3 -> x4, other arithmetic: 0.72 us -> 4.29 us  [the longest x1 3.58 us: apply_limits(): oldest = jnp.stack([*near[::-1], block_in, *z2], axis=0)]
  transfers between devices with their start and end apart: 6 -> 8, of which waited for: 4 -> 4; matrix products, arithmetic and copies ran while one was open for 11% -> 14% of each run, Pallas kernels for 0% -> 0%
where the time goes in v1:
time: 303 us; the launch traced here: 302 us
  waiting for transfers between devices  138 us (46%)
  blocking collectives  63.1 us (21%)
  local copies, waits for them, and re-layouts  32.8 us (11%)
  matrix products  19.2 us (6%)
  starting transfers between devices  17.6 us (6%)
  other arithmetic  16.6 us (5%)
  between operations  14.6 us (5%)
    all_to_all x1, blocking collectives, expert_half(): lax.all_to_all(sending, 'ep', split_axis=1, concat_axis=1, tiled=True)  63.1 us
    all_gather x1, waiting for transfers between devices, expert_half(): received = lax.all_gather(arrived, 'tp', axis=0, tiled=True)  56.5 us
    all_to_all x1, waiting for transfers between devices, expert_half(): lax.all_to_all(summed, 'ep', split_axis=1, concat_axis=1, tiled=True)  50 us
    ppermute x2, waiting for transfers between devices, apply_limits(): near.append(lax.ppermute(near[-1] if near else block_in, axis_name, sheets))  28.8 us
    scatter x1, local copies, waits for them, and re-layouts, dispatch_rows(): table.at[slot_index.reshape(-1), flat.reshape(-1)]  9.28 us
    all_to_all x1, starting transfers between devices, expert_half(): lax.all_to_all(summed, 'ep', split_axis=1, concat_axis=1, tiled=True)  7.18 us
  transfers between devices with their start and end apart: 8, of which 4 were waited for; matrix products, arithmetic and copies ran while one was open for 14% of the time, Pallas kernels for 0%

profile of v1, /device:TPU:8, one launch (start us, length us, event | category | flops | bytes accessed | tf_op | source)
XLA Modules:
  0.0 302.2 jit_solution(9516516437188427487)
XLA Ops:
  9.5 1.8 multiply_reduce_fusion
  11.3 2.0 convert_element_type.215
  13.9 9.3 %scatter_fusion = s32[6,64]{1,0:T(8,128)S(1)} fusion(s32[6,64]{1,0:T(8,128)S(1)} %broadcast_in_dim.11, s32[192]{0:T(256)S(1)} %bitcast.130, s32[192]{0:T(256)S(1)} %and_select_fusion.1), kind=kCustom, calls=%fused_computation.3 | custom fusion | bytes 3840 | tf_op jit(solution)/shard_map/scatter | solution.py:119
  23.5 1.3 fusion.26
  24.8 2.5 gather_fusion.1
  28.2 63.1 %all_to_all.28 = bf16[6,64,2048]{2,0,1:T(8,128)(2,1)S(1)} all-to-all(bf16[6,64,2048]{2,0,1:T(8,128)(2,1)S(1)} %copy_select_fusion), channel_id=1, replica_groups=mesh['ep'=64,'tp'=4] {'ep'}, dimensions={1} | all-to-all | bytes 3145728 | tf_op jit(solution)/shard_map/all_to_all | solution.py:143
  91.4 2.0 copy.48
  93.4 1.6 collective-permute-start.1
  95.0 1.7 collective-permute-start.3
  98.7 1.9 collective-permute-start
  100.8 2.9 collective-permute-done
  103.7 1.0 maximum_convert_fusion
  104.7 28.8 %collective-permute-done.1 = bf16[1,256,2048]{2,1,0:T(8,128)(2,1)} collective-permute-done((bf16[1,256,2048]{2,1,0:T(8,128)(2,1)}, bf16[1,256,2048]{2,1,0:T(8,128)(2,1)}, u32[]{:S(2)}, u32[]{:S(2)}) %collective-permute-start.1) | collective-permute-done | bytes 1048608 | tf_op jit(solution)/shard_map/ppermute | solution.py:26
  133.5 1.6 collective-permute-start.2
  135.2 56.5 %all-gather.2.cloned.1.call-done = bf16[24,64,2048]{2,1,0:T(8,128)(2,1)} async-done(((bf16[6,64,2048]{2,1,0:T(8,128)(2,1)}), bf16[24,64,2048]{2,1,0:T(8,128)(2,1)}) %all-gather.2.cloned.1.call-update) | async-done | bytes 6291472 | tf_op jit(solution)/shard_map/all_gather | solution.py:144
  191.7 5.1 %fusion.23 = f32[24,64,256]{2,1,0:T(8,128)S(1)} fusion(bf16[24,64,2048]{2,1,0:T(8,128)(2,1)} %all-gather.2.cloned.1.call-done, bf16[1,2048,256]{2,1,0:T(8,128)(2,1)} %param.25), kind=kOutput, calls=%fused_computation.48 | convolution fusion | flops 1610612736 | bytes 8912896 | tf_op jit(solution)/shard_map/csed,edh->cseh/dot_general | solution.py:149
  196.8 4.2 %fusion.16 = bf16[24,64,1,256]{3,1,2,0:T(8,128)(2,1)} fusion(bf16[24,64,2048]{2,1,0:T(8,128)(2,1)S(1)} %copy-done.10, f32[24,64,256]{2,1,0:T(8,128)S(1)} %fusion.23, bf16[1,2048,256]{2,1,0:T(8,128)(2,1)} %param.26), kind=kOutput, calls=%fused_computation.34 | convolution fusion | flops 1612972032 | bytes 9699328 | tf_op jit(solution)/shard_map/csed,edh->cseh/dot_general | solution.py:150
  201.0 3.5 %all-to-all-start.1 = ((bf16[24,64,1,256]{3,1,2,0:T(8,128)(2,1)}), bf16[24,64,1,256]{3,1,2,0:T(8,128)(2,1)S(1)}, u32[]{:S(2)}, u32[]{:S(2)}) async-start(bf16[24,64,1,256]{3,1,2,0:T(8,128)(2,1)} %fusion.16), calls=%async_computation.2 | async-start | bytes 1572864 | tf_op jit(solution)/shard_map/all_to_all | solution.py:152
  204.6 3.2 %convolution_convert_fusion = bf16[512,2048]{1,0:T(8,128)(2,1)} fusion(bf16[256,2048]{1,0:T(8,128)(2,1)S(1)} %copy-done, f32[256]{0:T(256)S(1)} %convert_element_type.211, f32[527,256]{1,0:T(8,128)S(1)} %maximum_convert_fusion, f32[512]{0:T(512)S(1)} %minimum_convert_fusion, f32[]{:T(128)S(6)} %convert_element_type.208, f32[]{:T(128)S(6)} %convert_element_type.207, ...), kind=kOutput, calls=%fused_computation.12 | convolution fusion | flops 609746944 | bytes 11668544 | tf_op jit(solution)/shard_map/dot_general | solution.py:96
  207.9 1.2 copy-done.4
  209.0 3.6 %maximum_bitcast_fusion = bf16[4,256,2048]{2,1,0:T(8,128)(2,1)} fusion(bf16[1,1,256,2048]{3,2,1,0:T(8,128)(2,1)} %bitcast.4, bf16[1,1,256,2048]{3,2,1,0:T(8,128)(2,1)S(1)} %bitcast.138, bf16[1,1,256,2048]{3,2,1,0:T(8,128)(2,1)} %bitcast.2, bf16[1,1,256,2048]{3,2,1,0:T(8,128)(2,1)} %bitcast.1), kind=kLoop, calls=%fused_computation.9 | loop fusion | flops 6291456 | bytes 8388608 | tf_op jit(solution)/shard_map/stack | solution.py:29
  212.6 5.0 %gather_fusion = bf16[4,256,2048]{2,1,0:T(8,128)(2,1)} fusion(bf16[4,256,2048]{2,1,0:T(8,128)(2,1)} %maximum_bitcast_fusion, s32[1024]{0:T(1024)S(1)} %pad_clamp_fusion.2), kind=kCustom, calls=%fused_computation | custom fusion | bytes 8388624 | tf_op jit(solution)/shard_map/gather | solution.py:31
  218.8 2.0 fusion.3
  220.7 1.8 fusion.4
  223.7 1.4 fusion.11
  225.1 2.2 copy.51
  227.3 7.2 %all-to-all-start.2 = ((bf16[6,64,2048]{2,0,1:T(8,128)(2,1)}), bf16[6,64,2048]{2,0,1:T(8,128)(2,1)}, u32[]{:S(2)}, u32[]{:S(2)}) async-start(bf16[6,64,2048]{2,0,1:T(8,128)(2,1)} %copy.51), calls=%async_computation.3 | async-start | bytes 4194304 | tf_op jit(solution)/shard_map/all_to_all | solution.py:165
  235.7 50.0 %all-to-all-done.2 = bf16[6,64,2048]{2,0,1:T(8,128)(2,1)} async-done(((bf16[6,64,2048]{2,0,1:T(8,128)(2,1)}), bf16[6,64,2048]{2,0,1:T(8,128)(2,1)}, u32[]{:S(2)}, u32[]{:S(2)}) %all-to-all-start.2) | async-done | bytes 1572896 | tf_op jit(solution)/shard_map/all_to_all | solution.py:165
  285.6 2.5 copy.52
  288.1 2.0 gather_fusion.2
  290.1 2.1 reshape.605
  292.3 3.1 %multiply_reduce_fusion.1 = bf16[96,2048]{1,0:T(8,128)(2,1)} fusion(f32[96,2,2048]{2,1,0:T(2,128)S(1)} %reshape.605, f32[96,2]{1,0:T(8,128)S(1)} %copy.53), kind=kLoop, calls=%fused_computation.33 | loop fusion | flops 589824 | bytes 1966848 | tf_op jit(solution)/shard_map/reduce_sum | solution.py:174
  (85 shorter events, 9.6 us)
Async XLA Ops:
  7.2 197.4 %copy-start = (bf16[256,2048]{1,0:T(8,128)(2,1)S(1)}, bf16[256,2048]{1,0:T(8,128)(2,1)}, u32[]{:S(2)}) copy-start(bf16[256,2048]{1,0:T(8,128)(2,1)} %param.19) | copy-start | bytes 3145732
  7.2 4.2 %copy-start.1 = (bf16[384,2048]{1,0:T(8,128)(2,1)S(1)}, bf16[384,2048]{1,0:T(8,128)(2,1)}, u32[]{:S(2)}) copy-start(bf16[384,2048]{1,0:T(8,128)(2,1)} %param.20) | copy-start | bytes 4718596
  7.2 184.5 %all-gather.2.cloned.1.call-start = ((), (), s32[]{:S(2)}) async-start(), calls=%async_computation.5 | async-start | bytes 7864320 | tf_op jit(solution)/shard_map/all_gather | solution.py:144
  13.4 10.0 %copy-start.8 = (bf16[2048]{0:T(1024)(128)(2,1)S(1)}, bf16[2048]{0:T(1024)(128)(2,1)}, u32[]{:S(2)}) copy-start(bf16[2048]{0:T(1024)(128)(2,1)} %param.21) | copy-start | bytes 12292
  91.4 5.4 %copy-start.3 = (bf16[512,2048]{1,0:T(8,128)(2,1)S(1)}, bf16[512,2048]{1,0:T(8,128)(2,1)}, u32[]{:S(2)}) copy-start(bf16[512,2048]{1,0:T(8,128)(2,1)} %param.14) | copy-start | bytes 6291460
  93.4 3.8 %copy-start.9 = (bf16[2048]{0:T(1024)(128)(2,1)S(1)}, bf16[2048]{0:T(1024)(128)(2,1)}, u32[]{:S(2)}) copy-start(bf16[2048]{0:T(1024)(128)(2,1)} %param.15) | copy-start | bytes 12292
  93.4 3.8 %copy-start.11 = (bf16[2048,256]{1,0:T(8,128)(2,1)S(1)}, bf16[2048,256]{1,0:T(8,128)(2,1)}, u32[]{:S(2)}) copy-start(bf16[2048,256]{1,0:T(8,128)(2,1)} %param.16) | copy-start | bytes 3145732
  93.4 40.1 %collective-permute-start.1 = (bf16[1,256,2048]{2,1,0:T(8,128)(2,1)}, bf16[1,256,2048]{2,1,0:T(8,128)(2,1)}, u32[]{:S(2)}, u32[]{:S(2)}) collective-permute-start(bf16[1,256,2048]{2,1,0:T(8,128)(2,1)} %param.27), channel_id=1, source_target_pairs={{0,1},{1,2},{2,3},{3,0},{4,5},{5,6},{6,7},{7,4},{8,9},{9,10},{10,1... | collective-permute-start | bytes 3145736 | tf_op jit(solution)/shard_map/ppermute | solution.py:26
  95.0 112.9 %collective-permute-start.3 = (bf16[1,256,2048]{2,1,0:T(8,128)(2,1)}, bf16[1,256,2048]{2,1,0:T(8,128)(2,1)}, u32[]{:S(2)}, u32[]{:S(2)}) collective-permute-start(bf16[1,256,2048]{2,1,0:T(8,128)(2,1)} %param.27), channel_id=1, source_target_pairs={{1,0},{2,1},{3,2},{0,3},{5,4},{6,5},{7,6},{4,7},{9,8},{10,9},{11,1... | collective-permute-start | bytes 3145736 | tf_op jit(solution)/shard_map/ppermute | solution.py:28
  97.2 3.5 %copy-start.13 = (bf16[256]{0:T(256)(128)(2,1)S(1)}, bf16[256]{0:T(256)(128)(2,1)}, u32[]{:S(2)}) copy-start(bf16[256]{0:T(256)(128)(2,1)} %param.18) | copy-start | bytes 1540
  98.0 0.7 copy-start.5
  98.7 5.0 %collective-permute-start = (bf16[15,256]{1,0:T(8,128)(2,1)S(1)}, bf16[15,256]{1,0:T(8,128)(2,1)S(1)}, u32[]{:S(2)}, u32[]{:S(2)}) collective-permute-start(bf16[15,256]{1,0:T(8,128)(2,1)S(1)} %slice.137), channel_id=1, source_target_pairs={{0,4},{4,8},{8,12},{12,16},{16,20},{20,24},{24,28},{28,32},{32,36}... | collective-permute-start | bytes 23048 | tf_op jit(solution)/shard_map/ppermute | solution.py:41
  133.5 74.3 %collective-permute-start.2 = (bf16[1,256,2048]{2,1,0:T(8,128)(2,1)}, bf16[1,256,2048]{2,1,0:T(8,128)(2,1)}, u32[]{:S(2)}, u32[]{:S(2)}) collective-permute-start(bf16[1,256,2048]{2,1,0:T(8,128)(2,1)} %collective-permute-done.1), channel_id=1, source_target_pairs={{0,1},{1,2},{2,3},{3,0},{4,5},{5,6},{6,7},{7,4},{8,9},{9,10},{10,1... | collective-permute-start | bytes 3145736 | tf_op jit(solution)/shard_map/ppermute | solution.py:26
  191.7 5.1 %copy-start.10 = (bf16[24,64,2048]{2,1,0:T(8,128)(2,1)S(1)}, bf16[24,64,2048]{2,1,0:T(8,128)(2,1)}, u32[]{:S(2)}) copy-start(bf16[24,64,2048]{2,1,0:T(8,128)(2,1)} %all-gather.2.cloned.1.call-done) | copy-start | bytes 18874372
  196.8 7.8 %copy-start.12 = (bf16[1,256,256]{2,1,0:T(8,128)(2,1)S(1)}, bf16[1,256,256]{2,1,0:T(8,128)(2,1)}, u32[]{:S(2)}) copy-start(bf16[1,256,256]{2,1,0:T(8,128)(2,1)} %param.17) | copy-start | bytes 393220
  201.0 16.6 %all-to-all-start.1 = ((bf16[24,64,1,256]{3,1,2,0:T(8,128)(2,1)}), bf16[24,64,1,256]{3,1,2,0:T(8,128)(2,1)S(1)}, u32[]{:S(2)}, u32[]{:S(2)}) async-start(bf16[24,64,1,256]{3,1,2,0:T(8,128)(2,1)} %fusion.16), calls=%async_computation.2 | async-start | bytes 1572864 | tf_op jit(solution)/shard_map/all_to_all | solution.py:152
  204.5 90.8 %reduce-scatter.2.cloned.1.call-start = ((), (), s32[]{:S(2)}) async-start(), calls=%async_computation.4 | async-start | bytes 2621440 | tf_op jit(solution)/shard_map/reduce_scatter | solution.py:95
  207.8 1.2 copy-start.4
  218.8 3.8 %copy-start.2 = (bf16[4,256,2048]{2,1,0:T(8,128)(2,1)S(1)}, bf16[4,256,2048]{2,1,0:T(8,128)(2,1)}, u32[]{:S(2)}) copy-start(bf16[4,256,2048]{2,1,0:T(8,128)(2,1)} %gather_fusion) | copy-start | bytes 12582916
  227.3 7.2 %copy-start.7 = (bf16[2048,4]{0,1:T(4,128)(2,1)S(1)}, bf16[2048,4]{0,1:T(4,128)(2,1)}, u32[]{:S(2)}) copy-start(bf16[2048,4]{0,1:T(4,128)(2,1)} %param.22) | copy-start | bytes 49156
  227.3 7.4 %copy-start.6 = (bf16[2048,64]{0,1:T(8,128)(2,1)S(1)}, bf16[2048,64]{0,1:T(8,128)(2,1)}, u32[]{:S(2)}) copy-start(bf16[2048,64]{0,1:T(8,128)(2,1)} %param.23) | copy-start | bytes 786436
  227.3 58.3 %all-to-all-start.2 = ((bf16[6,64,2048]{2,0,1:T(8,128)(2,1)}), bf16[6,64,2048]{2,0,1:T(8,128)(2,1)}, u32[]{:S(2)}, u32[]{:S(2)}) async-start(bf16[6,64,2048]{2,0,1:T(8,128)(2,1)} %copy.51), calls=%async_computation.3 | async-start | bytes 4194304 | tf_op jit(solution)/shard_map/all_to_all | solution.py:165
Sparse Core Ops, SparseCore 0:
  93.5 98.1 all-gather.1
  208.4 30.2 reduce-scatter.1
